TPU v7x, 32 devices: a whole 2x2x4 slice. The times are simulated.
32 devices in a mesh: rep: 2 (over x), fs: 8 (over z, y), tp: 2 (over core).
Axes of the slice: x: 2, y: 2, z: 4, core: 2. Of those that a mesh axis runs over, the one named last changes fastest.
Arguments:
- inputs: bfloat16 [8192, 2048], P(('rep', 'fs')), may hold values from -6 to 6
- gain: float32 [2048], replicated, may hold values from 0.1 to 1.9
- gate_weight: bfloat16 [2048, 3072], P('fs', 'tp'), may hold values from -0.125 to 0.125
- up_weight: bfloat16 [2048, 3072], P('fs', 'tp'), may hold values from -0.125 to 0.125
- down_weight: bfloat16 [2048, 3072], P('fs', 'tp'), may hold values from -0.109375 to 0.109375
- cotangent: bfloat16 [8192, 2048], P(('rep', 'fs')), may hold values from -6 to 6
Outputs:
- input_gradient: bfloat16 [8192, 2048], P(('rep', 'fs'))
- gain_gradient: float32 [2048], replicated
- d_down: float32 [2048, 3072], P('fs', 'tp')
All inputs are finite; a program needn't handle non-finite values.
Results may differ from a plain program's by a relative error of at most 0.014.
Values may be sent and summed in bfloat16 or wider, within the bound.
A program may use at most 128 MiB of HBM per device.

v0:
```python
import jax
import jax.numpy as jnp
from jax import lax
from jax.sharding import PartitionSpec as P

EPS = 1e-06


def local(inputs, gain, gate_weight, up_weight, down_weight, cotangent):
    single_precision = inputs.astype(jnp.float32)
    reciprocal_root_mean = lax.rsqrt(
        jnp.mean(single_precision * single_precision, axis=-1, keepdims=True) + EPS
    )
    unit_input = single_precision * reciprocal_root_mean
    normalized_input = (unit_input * gain).astype(jnp.bfloat16)
    row_count = inputs.shape[0]
    contract_cols = (((1,), (1,)), ((), ()))
    gate_full, up_full, down_full = (
        lax.all_gather(gate_weight, "fs", axis=0, tiled=True),
        lax.all_gather(up_weight, "fs", axis=0, tiled=True),
        lax.all_gather(down_weight, "fs", axis=0, tiled=True),
    )
    gate = jnp.dot(normalized_input, gate_full, preferred_element_type=jnp.float32)
    up_proj = jnp.dot(normalized_input, up_full, preferred_element_type=jnp.float32)
    down_sum = jnp.dot(cotangent, down_full, preferred_element_type=jnp.float32)
    gate_sig = jax.nn.sigmoid(gate)
    active = gate * gate_sig
    hidden = (active * up_proj).astype(jnp.bfloat16)
    d_hidden = 0.5 * down_sum
    d_gate = (d_hidden * up_proj * gate_sig * (1.0 + gate * (1.0 - gate_sig))).astype(jnp.bfloat16)
    d_up = (d_hidden * active).astype(jnp.bfloat16)
    partial_value = lax.dot_general(
        d_gate, gate_full, contract_cols, preferred_element_type=jnp.float32
    ) + lax.dot_general(d_up, up_full, contract_cols, preferred_element_type=jnp.float32)
    summed_units = lax.psum(partial_value.astype(jnp.bfloat16), "tp")
    normalized_gradient = summed_units.astype(jnp.float32)
    gain_gradient = lax.psum(jnp.sum(normalized_gradient * unit_input, axis=0), ("rep", "fs"))
    gain_scaled = gain * normalized_gradient
    mean_correction = jnp.mean(gain_scaled * unit_input, axis=-1, keepdims=True)
    input_gradient = (
        cotangent.astype(jnp.float32)
        + reciprocal_root_mean * (gain_scaled - unit_input * mean_correction)
    ).astype(jnp.bfloat16)
    contract_rows = (((0,), (0,)), ((), ()))
    width = cotangent.shape[1]
    groups_fs = lax.axis_size("fs")
    groups_rep = lax.axis_size("rep")
    sub_rows = width // (groups_fs * groups_rep)
    reordered = (
        cotangent.reshape(row_count, groups_fs, groups_rep, sub_rows)
        .transpose(0, 2, 1, 3)
        .reshape(row_count, width)
    )
    summed = lax.psum_scatter(
        0.5 * lax.dot_general(reordered, hidden, contract_rows, preferred_element_type=jnp.float32),
        ("rep", "fs"),
        scatter_dimension=0,
        tiled=True,
    )
    d_down = lax.all_gather(summed, "rep", axis=0, tiled=True)
    return (input_gradient, gain_gradient, d_down)


def solution(mesh):
    placed = (
        P(("rep", "fs"), None),
        P(),
        P("fs", "tp"),
        P("fs", "tp"),
        P("fs", "tp"),
        P(("rep", "fs"), None),
    )
    return jax.shard_map(
        local,
        mesh=mesh,
        in_specs=placed,
        out_specs=(P(("rep", "fs"), None), P(), P("fs", "tp")),
        check_vma=False,
    )
```

profile of v0, /device:TPU:0, one launch (start us, length us, event | category | flops | bytes accessed | tf_op | source)
XLA Modules:
  0.0 600.7 jit_solution(4841965839708579481)
XLA Ops:
  7.2 0.0 copy-start.1
  7.2 0.0 all-gather.9.cloned.1.call-start
  7.2 0.7 all-gather.9.cloned.1.call-update
  7.9 0.0 all-gather.7.cloned.1.call-start
  8.0 0.7 all-gather.7.cloned.1.call-update
  8.7 0.0 all-gather.5.cloned.1.call-start
  8.7 0.7 all-gather.5.cloned.1.call-update
  9.4 0.0 reduce-scatter.2.cloned.1.call-start
  9.4 0.0 copy-done.1
  9.5 2.5 copy.11
  12.0 0.0 copy-start
  12.0 0.0 copy-start.3
  12.0 3.3 copy.12
  15.2 0.0 copy-done
  15.2 0.5 fusion.9
  15.7 95.9 %all-gather.9.cloned.1.call-done = bf16[2048,1536]{1,0:T(8,128)(2,1)} async-done(((bf16[256,1536]{1,0:T(8,128)(2,1)}), bf16[2048,1536]{1,0:T(8,128)(2,1)}) %all-gather.9.cloned.1.call-update) | async-done | bytes 6291472 | tf_op jit(solution)/shard_map/all_gather | solution.py:19
  111.6 0.0 copy-done.3
  111.6 7.9 %fusion.14 = f32[512,1536]{1,0:T(8,128)} fusion(bf16[2048,1536]{1,0:T(8,128)(2,1)} %all-gather.9.cloned.1.call-done, bf16[512,2048]{1,0:T(8,128)(2,1)S(1)} %copy-done, f32[2048]{0:T(1024)S(1)} %copy-done.3, f32[512]{0:T(512)S(1)} %add_rsqrt_fusion), kind=kOutput, calls=%fused_computation.25 | convolution fusion | flops 3225419776 | bytes 11544576 | tf_op jit(solution)/shard_map/dot_general | solution.py:23
  119.5 91.2 %all-gather.7.cloned.1.call-done = bf16[2048,1536]{1,0:T(8,128)(2,1)} async-done(((bf16[256,1536]{1,0:T(8,128)(2,1)}), bf16[2048,1536]{1,0:T(8,128)(2,1)}) %all-gather.7.cloned.1.call-update) | async-done | bytes 6291472 | tf_op jit(solution)/shard_map/all_gather | solution.py:20
  210.7 0.0 copy-start.2
  210.7 0.0 copy-start.4
  210.7 5.8 fusion.16
  216.5 0.0 copy-start.6
  216.5 1.7 copy-done.6
  218.2 0.0 copy-done.2
  218.2 0.0 copy-done.4
  218.2 6.8 %multiply_bitcast_fusion = f32[2048,1536]{0,1:T(8,128)} fusion(bf16[512,2048]{0,1:T(8,128)(2,1)S(1)} %bitcast.14, f32[512,1536]{1,0:T(8,128)S(1)} %fusion.16, f32[512,1536]{1,0:T(8,128)S(1)} %copy-done.4), kind=kOutput, calls=%fused_computation | convolution fusion | flops 3229089792 | bytes 20971520 | tf_op jit(solution)/shard_map/dot_general | solution.py:55
  225.1 0.0 reduce-scatter.2.cloned.1.call-update
  225.1 0.2 all-reduce.2.cloned.1.call-start
  225.3 84.5 %all-gather.5.cloned.1.call-done = bf16[2048,1536]{1,0:T(8,128)(2,1)} async-done(((bf16[256,1536]{1,0:T(8,128)(2,1)}), bf16[2048,1536]{1,0:T(8,128)(2,1)}) %all-gather.5.cloned.1.call-update) | async-done | bytes 6291472 | tf_op jit(solution)/shard_map/all_gather | solution.py:21
  309.8 0.0 copy-start.5
  309.8 0.0 slice-start
  309.8 8.6 %convolution_multiply_fusion = f32[512,1536]{1,0:T(8,128)} fusion(bf16[512,2048]{1,0:T(8,128)(2,1)} %param.11, bf16[2048,1536]{1,0:T(8,128)(2,1)} %all-gather.5.cloned.1.call-done), kind=kOutput, calls=%fused_computation.17 | convolution fusion | flops 3222011904 | bytes 11534336 | tf_op jit(solution)/shard_map/dot_general | solution.py:25
  318.4 0.0 copy-done.5
  318.4 0.0 copy-done.7
  318.4 8.6 %fusion.12 = f32[512,2048]{1,0:T(8,128)S(1)} fusion(bf16[2048,1536]{1,0:T(8,128)(2,1)} %all-gather.9.cloned.1.call-done, f32[512,1536]{1,0:T(8,128)S(1)} %copy-done.5, f32[512,1536]{1,0:T(8,128)} %convolution_multiply_fusion, f32[512,1536]{1,0:T(8,128)S(1)} %copy-done.7), kind=kOutput, calls=%fused_computation.23 | convolution fusion | flops 3229089792 | bytes 19922944 | tf_op jit(solution)/shard_map/dot_general | solution.py:32
  327.0 0.0 slice-done
  327.0 0.0 slice-done.1
  327.1 6.6 %add_convert_fusion = bf16[512,2048]{1,0:T(8,128)(2,1)} fusion(f32[512,2048]{1,0:T(8,128)S(1)} %fusion.12, bf16[2048,1536]{1,0:T(8,128)(2,1)S(1)} %bitcast.16, f32[512,1536]{1,0:T(8,128)} %convolution_multiply_fusion, f32[512,1536]{1,0:T(8,128)S(1)} %copy-done.5), kind=kOutput, calls=%fused_computation.16 | convolution fusion | flops 3228041216 | bytes 18874368 | tf_op jit(solution)/shard_map/dot_general | solution.py:34
  333.7 0.0 all-reduce.2.cloned.1.call-update
  333.7 0.0 all-gather.11.cloned.1.call-start
  333.7 182.3 %reduce-scatter.2.cloned.1.call-done = f32[128,1536]{0,1:T(8,128)} async-done(((f32[2048,1536]{0,1:T(8,128)}), f32[128,1536]{0,1:T(8,128)}) %reduce-scatter.2.cloned.1.call-update) | async-done | bytes 786448 | tf_op jit(solution)/shard_map/reduce_scatter | solution.py:54
  516.0 0.0 all-gather.11.cloned.1.call-update
  516.1 23.6 %all-reduce.2.cloned.1.call-done = bf16[512,2048]{1,0:T(8,128)(2,1)} async-done(((bf16[512,2048]{1,0:T(8,128)(2,1)}), bf16[512,2048]{1,0:T(8,128)(2,1)}) %all-reduce.2.cloned.1.call-update) | async-done | bytes 2097168 | tf_op jit(solution)/shard_map/psum | solution.py:35
  539.6 2.9 fusion.10
  542.5 43.3 %psum.15 = f32[2048]{0:T(1024)} all-reduce(f32[2048]{0:T(1024)S(1)} %get-tuple-element.12), channel_id=1, replica_groups=mesh['rep'=2,'fs'=8,'tp'=2] {'rep','fs'}, use_global_device_ids=true, to_apply=%region_4.0 | all-reduce | flops 2048 | bytes 16384 | tf_op jit(solution)/shard_map/psum | solution.py:37
  585.8 5.0 fusion.6
  590.8 3.0 copy.13
  (6 shorter events, 0.0 us)
Async XLA Ops:
  7.2 2.3 copy-start.1
  7.2 104.4 %all-gather.9.cloned.1.call-start = ((), (), s32[]{:S(2)}) async-start(), calls=%async_computation.3 | async-start | bytes 7077888 | tf_op jit(solution)/shard_map/all_gather | solution.py:19
  7.9 202.8 %all-gather.7.cloned.1.call-start = ((), (), s32[]{:S(2)}) async-start(), calls=%async_computation.2 | async-start | bytes 7077888 | tf_op jit(solution)/shard_map/all_gather | solution.py:20
  8.7 301.1 %all-gather.5.cloned.1.call-start = ((), (), s32[]{:S(2)}) async-start(), calls=%async_computation.1 | async-start | bytes 7077888 | tf_op jit(solution)/shard_map/all_gather | solution.py:21
  9.4 506.6 %reduce-scatter.2.cloned.1.call-start = ((), (), s32[]{:S(2)}) async-start(), calls=%async_computation.5 | async-start | bytes 13369344 | tf_op jit(solution)/shard_map/reduce_scatter | solution.py:54
  12.0 3.3 copy-start
  12.0 99.7 %copy-start.3 = (f32[2048]{0:T(1024)S(1)}, f32[2048]{0:T(1024)}, u32[]{:S(2)}) copy-start(f32[2048]{0:T(1024)} %param.7) | copy-start | bytes 24580
  210.7 7.5 %copy-start.2 = (bf16[512,2,8,128]{0,3,2,1:T(8,128)(2,1)S(1)}, bf16[512,2,8,128]{0,3,2,1:T(8,128)(2,1)}, u32[]{:S(2)}) copy-start(bf16[512,2,8,128]{0,3,2,1:T(8,128)(2,1)} %copy.12) | copy-start | bytes 6291460
  210.7 7.5 %copy-start.4 = (f32[512,1536]{1,0:T(8,128)S(1)}, f32[512,1536]{1,0:T(8,128)}, u32[]{:S(2)}) copy-start(f32[512,1536]{1,0:T(8,128)} %fusion.14) | copy-start | bytes 9437188
  216.5 1.8 copy-start.6
  225.1 314.5 %all-reduce.2.cloned.1.call-start = ((), (), s32[]{:S(2)}) async-start(), calls=%async_computation.4 | async-start | bytes 4194304 | tf_op jit(solution)/shard_map/psum | solution.py:35
  309.8 8.6 %copy-start.5 = (f32[512,1536]{1,0:T(8,128)S(1)}, f32[512,1536]{1,0:T(8,128)}, u32[]{:S(2)}) copy-start(f32[512,1536]{1,0:T(8,128)} %fusion.14) | copy-start | bytes 9437188
  309.8 8.6 %copy-start.7 = (f32[512,1536]{1,0:T(8,128)S(1)}, f32[512,1536]{1,0:T(8,128)}, u32[]{:S(2)}) copy-start(f32[512,1536]{1,0:T(8,128)} %copy-done.6) | copy-start | bytes 9437188
  309.8 17.2 %slice-start = ((s8[6291456]{0:T(1024)(128)(4,1)}), s8[4194304]{0:T(1024)(128)(4,1)S(1)}, s32[]{:S(2)}) async-start(s8[6291456]{0:T(1024)(128)(4,1)} %bitcast.15), calls=%async_computation.7 | async-start | bytes 8388608
  318.4 8.6 %slice-start.1 = ((s8[6291456]{0:T(1024)(128)(4,1)}), s8[2097152]{0:T(1024)(128)(4,1)S(1)}, s32[]{:S(2)}) async-start(s8[6291456]{0:T(1024)(128)(4,1)} %bitcast.15), calls=%async_computation.8 | async-start | bytes 4194304
  333.7 257.1 %all-gather.11.cloned.1.call-start = ((), (), s32[]{:S(2)}) async-start(), calls=%async_computation.6 | async-start | bytes 2359296 | tf_op jit(solution)/shard_map/all_gather | solution.py:60
Sparse Core Ops, SparseCore 0:
  10.2 101.4 all-gather.8
  113.8 96.8 all-gather.6
  212.9 96.8 all-gather.4
  315.3 200.6 reduce-scatter.1
  518.8 20.7 all-reduce.1
  541.0 28.3 all-gather.10
where the time goes:
time: 601 us
  waiting for transfers between devices  480 us (80%)
  matrix products  44.2 us (7%)
  blocking collectives  43.3 us (7%)
  between operations  14.2 us (2%)
  local copies, waits for them, and re-layouts  10.6 us (2%)
  other arithmetic  8.39 us (1%)
    reduce_scatter x1, waiting for transfers between devices, local(): lax.psum_scatter(0.5 * lax.dot_general(reordered, hidden, contract_rows,...  182 us
    all_gather x1, waiting for transfers between devices, local(): lax.all_gather(gate_weight, 'fs', axis=0, tiled=True)  95.9 us
    all_gather x1, waiting for transfers between devices, local(): lax.all_gather(up_weight, 'fs', axis=0, tiled=True)  91.2 us
    all_gather x1, waiting for transfers between devices, local(): lax.all_gather(down_weight, 'fs', axis=0, tiled=True)  84.5 us
    psum x1, blocking collectives, local(): lax.psum(jnp.sum(normalized_gradient * unit_input, axis=0), ('rep', 'fs'))  43.3 us
    psum x1, waiting for transfers between devices, local(): summed_units = lax.psum(partial_value.astype(jnp.bfloat16), 'tp')  23.6 us
  transfers between devices with their start and end apart: 6, of which 5 were waited for; matrix products, arithmetic and copies ran while one was open for 10% of the time, Pallas kernels for 0%

commit v1 on v0

--- a/solution.py
+++ b/solution.py
@@ -4,6 +4,27 @@
 from jax.sharding import PartitionSpec as P
 
 EPS = 1e-06
+
+
+def ring_gather(array, axis, dim):
+    size, mine, rows = (lax.axis_size(axis), lax.axis_index(axis), array.shape[dim])
+    ahead = [(i, (i + 1) % size) for i in range(size)]
+    left = [(i, (i - 1) % size) for i in range(size)]
+    filled = jnp.zeros((*array.shape[:dim], size * rows, *array.shape[dim + 1 :]), array.dtype)
+    filled = lax.dynamic_update_slice_in_dim(filled, array, mine * rows, axis=dim)
+    from_left = from_right = array
+    middle = size // 2
+    for hop in range(1, middle + 1):
+        from_left = lax.ppermute(from_left, axis, ahead)
+        filled = lax.dynamic_update_slice_in_dim(
+            filled, from_left, (mine - hop) % size * rows, axis=dim
+        )
+        if hop < size - middle:
+            from_right = lax.ppermute(from_right, axis, left)
+            filled = lax.dynamic_update_slice_in_dim(
+                filled, from_right, (mine + hop) % size * rows, axis=dim
+            )
+    return filled
 
 
 def local(inputs, gain, gate_weight, up_weight, down_weight, cotangent):
@@ -17,7 +38,7 @@
     contract_cols = (((1,), (1,)), ((), ()))
     gate_full, up_full, down_full = (
         lax.all_gather(gate_weight, "fs", axis=0, tiled=True),
-        lax.all_gather(up_weight, "fs", axis=0, tiled=True),
+        ring_gather(up_weight, "fs", 0),
         lax.all_gather(down_weight, "fs", axis=0, tiled=True),
     )
     gate = jnp.dot(normalized_input, gate_full, preferred_element_type=jnp.float32)

time: 601 us -> 581 us (0.967)
  waiting for transfers between devices: 480 us -> 432 us
  starting transfers between devices: 0.42 us -> 21.9 us
  local copies, waits for them, and re-layouts: 10.6 us -> 18.3 us
    ppermute x0 -> x7, waiting for transfers between devices: none -> 147 us  [the longest x4 141 us: ring_gather(): from_left = lax.ppermute(from_left, axis, ahead)]
    all_gather x1, waiting for transfers between devices: 95.9 us -> 0.01 us  [local(): lax.all_gather(gate_weight, 'fs', axis=0, tiled=True)]
    all_gather x1 -> x0, waiting for transfers between devices: 91.2 us -> none  [local(): lax.all_gather(up_weight, 'fs', axis=0, tiled=True)]
    ppermute x0 -> x7, starting transfers between devices: none -> 21.5 us  [the longest x3 11 us: ring_gather(): from_right = lax.ppermute(from_right, axis, left)]
    all_gather x1, waiting for transfers between devices: 84.5 us -> 76.6 us  [local(): lax.all_gather(down_weight, 'fs', axis=0, tiled=True)]
  transfers between devices with their start and end apart: 6 -> 12, of which waited for: 5 -> 8; matrix products, arithmetic and copies ran while one was open for 10% -> 11% of each run, Pallas kernels for 0% -> 0%
where the time goes in v1:
time: 581 us
  waiting for transfers between devices  432 us (74%)
  blocking collectives  43.3 us (7%)
  matrix products  41.7 us (7%)
  starting transfers between devices  21.9 us (4%)
  local copies, waits for them, and re-layouts  18.3 us (3%)
  between operations  13.9 us (2%)
  other arithmetic  9.98 us (2%)
    reduce_scatter x1, waiting for transfers between devices, local(): lax.psum_scatter(0.5 * lax.dot_general(reordered, hidden, contract_rows,...  183 us
    ppermute x4, waiting for transfers between devices, ring_gather(): from_left = lax.ppermute(from_left, axis, ahead)  141 us
    all_gather x1, waiting for transfers between devices, local(): lax.all_gather(down_weight, 'fs', axis=0, tiled=True)  76.6 us
    psum x1, blocking collectives, local(): lax.psum(jnp.sum(normalized_gradient * unit_input, axis=0), ('rep', 'fs'))  43.3 us
    psum x1, waiting for transfers between devices, local(): summed_units = lax.psum(partial_value.astype(jnp.bfloat16), 'tp')  23.6 us
  transfers between devices with their start and end apart: 12, of which 8 were waited for; matrix products, arithmetic and copies ran while one was open for 11% of the time, Pallas kernels for 0%

profile of v1, /device:TPU:0, one launch (start us, length us, event | category | flops | bytes accessed | tf_op | source)
XLA Modules:
  0.0 580.6 jit_solution(8786182151702985928)
XLA Ops:
  7.2 0.0 all-gather.6.cloned.1.call-start
  7.2 0.7 all-gather.6.cloned.1.call-update
  7.9 0.0 all-gather.4.cloned.1.call-start
  8.0 0.7 all-gather.4.cloned.1.call-update
  8.7 0.0 reduce-scatter.2.cloned.1.call-start
  8.7 3.0 collective-permute-start
  11.8 3.1 collective-permute-start.1
  14.9 39.3 %collective-permute-done = bf16[256,1536]{1,0:T(8,128)(2,1)S(1)} collective-permute-done((bf16[256,1536]{1,0:T(8,128)(2,1)}, bf16[256,1536]{1,0:T(8,128)(2,1)S(1)}, u32[]{:S(2)}, u32[]{:S(2)}) %collective-permute-start) | collective-permute-done | bytes 786464 | tf_op jit(solution)/shard_map/ppermute | solution.py:18
  54.2 2.4 collective-permute-start.2
  56.5 3.9 collective-permute-start.3
  60.4 2.1 fusion.9
  62.5 42.3 %collective-permute-done.2 = bf16[256,1536]{1,0:T(8,128)(2,1)} collective-permute-done((bf16[256,1536]{1,0:T(8,128)(2,1)S(1)}, bf16[256,1536]{1,0:T(8,128)(2,1)}, u32[]{:S(2)}, u32[]{:S(2)}) %collective-permute-start.2) | collective-permute-done | bytes 786464 | tf_op jit(solution)/shard_map/ppermute | solution.py:18
  104.8 2.6 collective-permute-start.4
  107.4 2.5 copy.11
  109.9 3.1 copy.12
  113.0 0.4 broadcast_in_dim.2
  113.4 0.7 copy-done.4
  114.2 0.1 constant_dynamic-update-slice_fusion.7
  114.2 0.2 copy-done.6
  114.4 0.1 constant_dynamic-update-slice_fusion.6
  114.5 4.0 collective-permute-start.5
  118.5 1.2 constant_dynamic-update-slice_fusion.5
  119.7 38.4 %collective-permute-done.4 = bf16[256,1536]{1,0:T(8,128)(2,1)} collective-permute-done((bf16[256,1536]{1,0:T(8,128)(2,1)}, bf16[256,1536]{1,0:T(8,128)(2,1)}, u32[]{:S(2)}, u32[]{:S(2)}) %collective-permute-start.4) | collective-permute-done | bytes 786464 | tf_op jit(solution)/shard_map/ppermute | solution.py:18
  158.1 2.5 collective-permute-start.6
  160.6 1.2 constant_dynamic-update-slice_fusion.4
  161.8 0.1 constant_dynamic-update-slice_fusion.3
  161.9 1.3 constant_dynamic-update-slice_fusion.2
  163.2 5.8 collective-permute-done.5
  169.0 0.1 constant_dynamic-update-slice_fusion.1
  169.0 21.4 %collective-permute-done.6 = bf16[256,1536]{1,0:T(8,128)(2,1)S(1)} collective-permute-done((bf16[256,1536]{1,0:T(8,128)(2,1)}, bf16[256,1536]{1,0:T(8,128)(2,1)S(1)}, u32[]{:S(2)}, u32[]{:S(2)}) %collective-permute-start.6) | collective-permute-done | bytes 786464 | tf_op jit(solution)/shard_map/ppermute | solution.py:18
  190.4 0.1 constant_dynamic-update-slice_fusion
  190.5 2.7 copy-done.2
  193.2 5.2 fusion.16
  198.4 6.0 %fusion.14 = f32[512,1536]{1,0:T(8,128)S(1)} fusion(bf16[2048,1536]{1,0:T(8,128)(2,1)} %all-gather.6.cloned.1.call-done, bf16[512,2048]{1,0:T(8,128)(2,1)S(1)} %copy-done, f32[2048]{0:T(1024)S(1)} %copy-done.7, f32[512]{0:T(512)S(1)} %add_rsqrt_fusion), kind=kOutput, calls=%fused_computation.25 | convolution fusion | flops 3225419776 | bytes 11544576 | tf_op jit(solution)/shard_map/dot_general | solution.py:44
  204.3 1.6 copy-done.10
  206.0 6.8 %multiply_bitcast_fusion = f32[2048,1536]{0,1:T(8,128)} fusion(bf16[512,2048]{0,1:T(8,128)(2,1)S(1)} %bitcast.16, f32[512,1536]{1,0:T(8,128)S(1)} %copy-done.8, f32[512,1536]{1,0:T(8,128)S(1)} %fusion.14), kind=kOutput, calls=%fused_computation | convolution fusion | flops 3229089792 | bytes 20971520 | tf_op jit(solution)/shard_map/dot_general | solution.py:76
  212.8 0.2 all-reduce.2.cloned.1.call-start
  213.1 76.6 %all-gather.4.cloned.1.call-done = bf16[2048,1536]{1,0:T(8,128)(2,1)} async-done(((bf16[256,1536]{1,0:T(8,128)(2,1)}), bf16[2048,1536]{1,0:T(8,128)(2,1)}) %all-gather.4.cloned.1.call-update) | async-done | bytes 6291472 | tf_op jit(solution)/shard_map/all_gather | solution.py:42
  289.7 8.6 %convolution_multiply_fusion = f32[512,1536]{1,0:T(8,128)} fusion(bf16[512,2048]{1,0:T(8,128)(2,1)} %param.11, bf16[2048,1536]{1,0:T(8,128)(2,1)} %all-gather.4.cloned.1.call-done), kind=kOutput, calls=%fused_computation.17 | convolution fusion | flops 3222011904 | bytes 11534336 | tf_op jit(solution)/shard_map/dot_general | solution.py:46
  298.3 8.5 %fusion.12 = f32[512,2048]{1,0:T(8,128)S(1)} fusion(bf16[2048,1536]{1,0:T(8,128)(2,1)} %all-gather.6.cloned.1.call-done, f32[512,1536]{1,0:T(8,128)S(1)} %copy-done.11, f32[512,1536]{1,0:T(8,128)} %convolution_multiply_fusion, f32[512,1536]{1,0:T(8,128)S(1)} %copy-done.9), kind=kOutput, calls=%fused_computation.23 | convolution fusion | flops 3229089792 | bytes 19922944 | tf_op jit(solution)/shard_map/dot_general | solution.py:53
  306.8 6.6 %add_convert_fusion = bf16[512,2048]{1,0:T(8,128)(2,1)} fusion(f32[512,2048]{1,0:T(8,128)S(1)} %fusion.12, bf16[2048,1536]{1,0:T(8,128)(2,1)S(1)} %bitcast.15, f32[512,1536]{1,0:T(8,128)} %convolution_multiply_fusion, f32[512,1536]{1,0:T(8,128)S(1)} %copy-done.11), kind=kOutput, calls=%fused_computation.16 | convolution fusion | flops 3228041216 | bytes 18874368 | tf_op jit(solution)/shard_map/dot_general | solution.py:55
  313.5 0.0 all-gather.8.cloned.1.call-start
  313.5 182.8 %reduce-scatter.2.cloned.1.call-done = f32[128,1536]{0,1:T(8,128)} async-done(((f32[2048,1536]{0,1:T(8,128)}), f32[128,1536]{0,1:T(8,128)}) %reduce-scatter.2.cloned.1.call-update) | async-done | bytes 786448 | tf_op jit(solution)/shard_map/reduce_scatter | solution.py:75
  496.3 23.6 %all-reduce.2.cloned.1.call-done = bf16[512,2048]{1,0:T(8,128)(2,1)} async-done(((bf16[512,2048]{1,0:T(8,128)(2,1)}), bf16[512,2048]{1,0:T(8,128)(2,1)}) %all-reduce.2.cloned.1.call-update) | async-done | bytes 2097168 | tf_op jit(solution)/shard_map/psum | solution.py:56
  519.9 2.9 fusion.10
  522.8 43.3 %psum.15 = f32[2048]{0:T(1024)} all-reduce(f32[2048]{0:T(1024)S(1)} %get-tuple-element.12), channel_id=1, replica_groups=mesh['rep'=2,'fs'=8,'tp'=2] {'rep','fs'}, use_global_device_ids=true, to_apply=%region_4.5 | all-reduce | flops 2048 | bytes 16384 | tf_op jit(solution)/shard_map/psum | solution.py:58
  566.1 5.0 fusion.6
  571.1 3.0 copy.13
  (34 shorter events, 0.1 us)
Async XLA Ops:
  7.2 100.3 %copy-start.1 = (bf16[512,2048]{1,0:T(8,128)(2,1)S(1)}, bf16[512,2048]{1,0:T(8,128)(2,1)}, u32[]{:S(2)}) copy-start(bf16[512,2048]{1,0:T(8,128)(2,1)} %param.11) | copy-start | bytes 6291460
  7.2 191.2 %all-gather.6.cloned.1.call-start = ((), (), s32[]{:S(2)}) async-start(), calls=%async_computation.2 | async-start | bytes 7077888 | tf_op jit(solution)/shard_map/all_gather | solution.py:40
  7.9 281.8 %all-gather.4.cloned.1.call-start = ((), (), s32[]{:S(2)}) async-start(), calls=%async_computation.1 | async-start | bytes 7077888 | tf_op jit(solution)/shard_map/all_gather | solution.py:42
  8.7 487.6 %reduce-scatter.2.cloned.1.call-start = ((), (), s32[]{:S(2)}) async-start(), calls=%async_computation.4 | async-start | bytes 13369344 | tf_op jit(solution)/shard_map/reduce_scatter | solution.py:75
  8.7 45.4 %collective-permute-start = (bf16[256,1536]{1,0:T(8,128)(2,1)}, bf16[256,1536]{1,0:T(8,128)(2,1)S(1)}, u32[]{:S(2)}, u32[]{:S(2)}) collective-permute-start(bf16[256,1536]{1,0:T(8,128)(2,1)} %param.9), channel_id=1, source_target_pairs={{0,2},{2,4},{4,6},{6,8},{8,10},{10,12},{12,14},{14,0},{1,3},{3,5},... | collective-permute-start | bytes 2359304 | tf_op jit(solution)/shard_map/ppermute | solution.py:18
  11.8 44.8 %collective-permute-start.1 = (bf16[256,1536]{1,0:T(8,128)(2,1)}, bf16[256,1536]{1,0:T(8,128)(2,1)}, u32[]{:S(2)}, u32[]{:S(2)}) collective-permute-start(bf16[256,1536]{1,0:T(8,128)(2,1)} %param.9), channel_id=1, source_target_pairs={{0,14},{2,0},{4,2},{6,4},{8,6},{10,8},{12,10},{14,12},{1,15},{3,1}... | collective-permute-start | bytes 2359304 | tf_op jit(solution)/shard_map/ppermute | solution.py:23
  54.1 2.4 copy-start.5
  54.2 50.7 %collective-permute-start.2 = (bf16[256,1536]{1,0:T(8,128)(2,1)S(1)}, bf16[256,1536]{1,0:T(8,128)(2,1)}, u32[]{:S(2)}, u32[]{:S(2)}) collective-permute-start(bf16[256,1536]{1,0:T(8,128)(2,1)S(1)} %collective-permute-done), channel_id=1, source_target_pairs={{0,2},{2,4},{4,6},{6,8},{8,10},{10,12},{12,14},{14,0},{1,3},{3,5},... | collective-permute-start | bytes 2359304 | tf_op jit(solution)/shard_map/ppermute | solution.py:18
  56.5 57.9 %collective-permute-start.3 = (bf16[256,1536]{1,0:T(8,128)(2,1)}, bf16[256,1536]{1,0:T(8,128)(2,1)S(1)}, u32[]{:S(2)}, u32[]{:S(2)}) collective-permute-start(bf16[256,1536]{1,0:T(8,128)(2,1)} %collective-permute-done.1), channel_id=1, source_target_pairs={{0,14},{2,0},{4,2},{6,4},{8,6},{10,8},{12,10},{14,12},{1,15},{3,1}... | collective-permute-start | bytes 2359304 | tf_op jit(solution)/shard_map/ppermute | solution.py:23
  104.8 53.3 %collective-permute-start.4 = (bf16[256,1536]{1,0:T(8,128)(2,1)}, bf16[256,1536]{1,0:T(8,128)(2,1)}, u32[]{:S(2)}, u32[]{:S(2)}) collective-permute-start(bf16[256,1536]{1,0:T(8,128)(2,1)} %collective-permute-done.2), channel_id=1, source_target_pairs={{0,2},{2,4},{4,6},{6,8},{8,10},{10,12},{12,14},{14,0},{1,3},{3,5},... | collective-permute-start | bytes 2359304 | tf_op jit(solution)/shard_map/ppermute | solution.py:18
  113.0 1.1 copy-start.4
  113.0 1.4 copy-start.6
  114.5 54.5 %collective-permute-start.5 = (bf16[256,1536]{1,0:T(8,128)(2,1)S(1)}, bf16[256,1536]{1,0:T(8,128)(2,1)S(1)}, u32[]{:S(2)}, u32[]{:S(2)}) collective-permute-start(bf16[256,1536]{1,0:T(8,128)(2,1)S(1)} %collective-permute-done.3), channel_id=1, source_target_pairs={{0,14},{2,0},{4,2},{6,4},{8,6},{10,8},{12,10},{14,12},{1,15},{3,1}... | collective-permute-start | bytes 2359304 | tf_op jit(solution)/shard_map/ppermute | solution.py:23
  158.1 32.3 %collective-permute-start.6 = (bf16[256,1536]{1,0:T(8,128)(2,1)}, bf16[256,1536]{1,0:T(8,128)(2,1)S(1)}, u32[]{:S(2)}, u32[]{:S(2)}) collective-permute-start(bf16[256,1536]{1,0:T(8,128)(2,1)} %collective-permute-done.4), channel_id=1, source_target_pairs={{0,2},{2,4},{4,6},{6,8},{8,10},{10,12},{12,14},{14,0},{1,3},{3,5},... | collective-permute-start | bytes 2359304 | tf_op jit(solution)/shard_map/ppermute | solution.py:18
  161.8 31.4 %copy-start = (bf16[512,2048]{1,0:T(8,128)(2,1)S(1)}, bf16[512,2048]{1,0:T(8,128)(2,1)}, u32[]{:S(2)}) copy-start(bf16[512,2048]{1,0:T(8,128)(2,1)} %param.6) | copy-start | bytes 6291460
  161.8 31.4 %copy-start.7 = (f32[2048]{0:T(1024)S(1)}, f32[2048]{0:T(1024)}, u32[]{:S(2)}) copy-start(f32[2048]{0:T(1024)} %param.7) | copy-start | bytes 24580
  190.5 2.7 copy-start.2
  198.4 7.6 %copy-start.3 = (bf16[512,2,8,128]{0,3,2,1:T(8,128)(2,1)S(1)}, bf16[512,2,8,128]{0,3,2,1:T(8,128)(2,1)}, u32[]{:S(2)}) copy-start(bf16[512,2,8,128]{0,3,2,1:T(8,128)(2,1)} %copy.12) | copy-start | bytes 6291460
  198.4 7.6 %copy-start.8 = (f32[512,1536]{1,0:T(8,128)S(1)}, f32[512,1536]{1,0:T(8,128)}, u32[]{:S(2)}) copy-start(f32[512,1536]{1,0:T(8,128)} %fusion.16) | copy-start | bytes 9437188
  204.3 1.6 copy-start.10
  212.8 307.0 %all-reduce.2.cloned.1.call-start = ((), (), s32[]{:S(2)}) async-start(), calls=%async_computation.3 | async-start | bytes 4194304 | tf_op jit(solution)/shard_map/psum | solution.py:56
  289.7 8.6 %copy-start.9 = (f32[512,1536]{1,0:T(8,128)S(1)}, f32[512,1536]{1,0:T(8,128)}, u32[]{:S(2)}) copy-start(f32[512,1536]{1,0:T(8,128)} %fusion.16) | copy-start | bytes 9437188
  289.7 8.6 %copy-start.11 = (f32[512,1536]{1,0:T(8,128)S(1)}, f32[512,1536]{1,0:T(8,128)}, u32[]{:S(2)}) copy-start(f32[512,1536]{1,0:T(8,128)} %copy-done.10) | copy-start | bytes 9437188
  289.7 17.1 %slice-start = ((s8[6291456]{0:T(1024)(128)(4,1)}), s8[4194304]{0:T(1024)(128)(4,1)S(1)}, s32[]{:S(2)}) async-start(s8[6291456]{0:T(1024)(128)(4,1)} %bitcast.14), calls=%async_computation.6 | async-start | bytes 8388608
  298.3 8.5 %slice-start.1 = ((s8[6291456]{0:T(1024)(128)(4,1)}), s8[2097152]{0:T(1024)(128)(4,1)S(1)}, s32[]{:S(2)}) async-start(s8[6291456]{0:T(1024)(128)(4,1)} %bitcast.14), calls=%async_computation.7 | async-start | bytes 4194304
  313.5 257.6 %all-gather.8.cloned.1.call-start = ((), (), s32[]{:S(2)}) async-start(), calls=%async_computation.5 | async-start | bytes 2359296 | tf_op jit(solution)/shard_map/all_gather | solution.py:81
Sparse Core Ops, SparseCore 0:
  10.2 179.9 all-gather.5
  192.3 97.2 all-gather.3
  295.3 200.9 reduce-scatter.1
  499.0 20.7 all-reduce.1
  521.2 28.3 all-gather.7
